TPU v7x, 32 devices: a whole 2x2x4 slice. The times are simulated.
32 devices in a mesh: grp: 2 (over y), ep: 8 (over z, core), tp: 2 (over x).
Axes of the slice: x: 2, y: 2, z: 4, core: 2. Of those that a mesh axis runs over, the one named last changes fastest.
Arguments:
- value_in: bfloat16 [8192, 1024], P(('grp', 'ep'), 'tp'), parts along dimension 0, may hold values from -6 to 6
- gate_in: bfloat16 [8192, 1024], P(('grp', 'ep'), 'tp'), parts along dimension 0, may hold values from -6 to 6
- conv_taps: float32 [31, 1024], P(None, 'tp'), may hold values from -12 to 12
- chan_gain: float32 [1024], replicated, may hold values from 0.1 to 1.9
- out_weight: bfloat16 [1024, 2048], P(None, 'tp'), may hold values from -0.1875 to 0.1875
- second_rows: bfloat16 [2048, 2048], P(('grp', 'ep')), parts along dimension 0, may hold values from -6 to 6
- expert_gain: float32 [2048], replicated, may hold values from 0.1 to 1.9
- routes: int32 [2048, 2], P(('grp', 'ep')), parts along dimension 0, may hold values from 0 to 3, all different within a row; in each aligned block of 128 rows (0 to 127, 128 to 255, ...) at most 96 rows name the same one
- route_weights: float32 [2048, 2], P(('grp', 'ep')), parts along dimension 0, may hold values from 0.1 to 0.9
- gate_w: bfloat16 [8, 2048, 2048], P('ep', None, 'tp'), may hold values from -0.125 to 0.125
- up_w: bfloat16 [8, 2048, 2048], P('ep', None, 'tp'), may hold values from -0.125 to 0.125
- down_w: bfloat16 [8, 2048, 2048], P('ep', 'tp'), may hold values from -0.125 to 0.125
Outputs:
- mixer_rows: bfloat16 [8192, 2048], P(('grp', 'ep'), 'tp'), parts along dimension 0
- routed_rows: bfloat16 [2048, 2048], P(('grp', 'ep'), 'tp'), parts along dimension 0
There are 2 independent parts, one for each index of `grp`. A program takes and returns all parts, laid end to end along the dimension named above; an argument that names none is the same for every part. Nothing has to cross between parts.
Inputs may be any that keep to these rules, and one draw needn't show every extreme that they name: `routes`: in each aligned block of 128 rows (the rows of one index of ep) no expert is named by more than 96 rows, a bound that some block reaches; each row names 2 different experts.
All inputs are finite; a program needn't handle non-finite values.
Results may differ from a plain program's by a relative error of at most 0.017.
Values may be sent and summed in bfloat16 or wider, within the bound.
A program may use at most 64 MiB of HBM per device.

v0:
```python
import functools

import jax
import jax.numpy as jnp
from jax import lax
from jax.experimental import pallas as pl
from jax.experimental.pallas import tpu as pltpu
from jax.sharding import PartitionSpec as P

eps = 1e-06
LANES = 128
MESH = pl.DeviceIdType.MESH


def partner_2(value, axis, bit):
    return lax.ppermute(value, axis, [(i, i ^ 1 << bit) for i in range(lax.axis_size(axis))])


def shifted(value, axis, by):
    devices = lax.axis_size(axis)
    pairs = [(i, i + by) for i in range(devices) if 0 <= i + by < devices]
    return lax.ppermute(value, axis, pairs)


def partner(block):
    return partner_2(block, "ep", 0)


def across(block):
    return lax.all_to_all(block, "ep", split_axis=0, concat_axis=0, tiled=True)


def on_device(
    value_in,
    gate_in,
    conv_taps,
    chan_gain,
    out_weight,
    second_rows,
    expert_gain,
    routes,
    route_weights,
    gate_w,
    up_w,
    down_w,
):
    taps = conv_taps.shape[0]
    glu = (value_in.astype(jnp.float32) * jax.nn.sigmoid(gate_in.astype(jnp.float32))).astype(
        jnp.bfloat16
    )
    length = glu.shape[0]
    before = shifted(glu[length - taps + 1 :], "ep", 1)
    padded = jnp.concatenate([before, glu], axis=0).astype(jnp.float32)
    total = jnp.zeros(glu.shape, jnp.float32)
    for offset in range(taps):
        total = total + conv_taps[offset][None, :] * padded[offset : offset + length]
    convolved = total.astype(jnp.bfloat16)
    channels = lax.all_gather(convolved, "tp", axis=1, tiled=True)
    values = channels.astype(jnp.float32)
    centered = values - jnp.mean(values, axis=-1, keepdims=True)
    scaled = (
        centered
        * lax.rsqrt(jnp.mean(centered * centered, axis=-1, keepdims=True) + eps)
        * chan_gain
    )
    activated = jax.nn.silu(scaled).astype(jnp.bfloat16)
    mixer_rows = jnp.dot(activated, out_weight, preferred_element_type=jnp.float32).astype(
        jnp.bfloat16
    )
    n_ep = lax.axis_size("ep")
    experts = n_ep // 2
    tokens = second_rows.shape[0]
    top = routes.shape[1]
    width = second_rows.shape[1]
    capacity = 2 * max(1, min(tokens // 2, 3 * tokens * top // (4 * experts)))
    half_slots = capacity // 2
    rows = second_rows.astype(jnp.float32)
    normed = (
        rows * lax.rsqrt(jnp.mean(rows * rows, axis=-1, keepdims=True) + eps) * expert_gain
    ).astype(jnp.bfloat16)
    chosen = routes.reshape(-1)
    hits = (chosen[:, None] == jnp.arange(experts, dtype=jnp.int32)[None, :]).astype(jnp.int32)
    place = jnp.sum((jnp.cumsum(hits, axis=0) - 1) * hits, axis=1)
    target = (chosen * capacity + place).reshape(tokens, top)
    slots = jnp.arange(experts * capacity, dtype=jnp.int32)
    matches = target[:, :, None] == slots[None, None, :]
    picker = jnp.any(matches, axis=1).astype(jnp.bfloat16)
    outgoing = jnp.dot(picker.T, normed, preferred_element_type=jnp.float32).astype(jnp.bfloat16)
    combiner = jnp.sum(jnp.where(matches, route_weights[:, :, None], 0.0), axis=1)
    upper = lax.axis_index("ep") % 2
    arrived = across(outgoing.reshape(n_ep, half_slots, width))
    other = partner(arrived)
    first = jnp.where(upper == 0, arrived, other)
    second = jnp.where(upper == 0, other, arrived)
    incoming = jnp.concatenate([first, second], axis=1)
    block_rows = incoming.reshape(n_ep * capacity, width)
    gate = jnp.dot(block_rows, gate_w[0], preferred_element_type=jnp.float32)
    lifted = jnp.dot(block_rows, up_w[0], preferred_element_type=jnp.float32)
    hidden = (jax.nn.silu(gate) * lifted).astype(jnp.bfloat16)
    partial_value = jnp.dot(hidden, down_w[0], preferred_element_type=jnp.float32)
    half_sums = lax.psum_scatter(
        partial_value.astype(jnp.bfloat16), "tp", scatter_dimension=1, tiled=True
    )
    columns = half_sums.shape[1]
    half_sums = half_sums.reshape(n_ep, capacity, columns)
    other_sums = partner(half_sums)
    joined = (half_sums.astype(jnp.float32) + other_sums.astype(jnp.float32)).astype(jnp.bfloat16)
    own = lax.dynamic_slice_in_dim(joined, upper * half_slots, half_slots, 1)
    results = across(own).reshape(experts * capacity, columns)
    routed_rows = jnp.dot(
        combiner,
        results.astype(jnp.float32),
        precision=lax.Precision.HIGHEST,
        preferred_element_type=jnp.float32,
    ).astype(jnp.bfloat16)
    return (mixer_rows, routed_rows)


def _xor(value, mask):
    out, bit = value, 1
    while bit <= mask:
        if mask & bit:
            out = out + bit - 2 * bit * lax.rem(lax.div(value, bit), 2)
        bit *= 2
    return out


def _iota(shape, dim):
    return lax.broadcasted_iota(jnp.int32, shape, dim)


def _dot(a, b):
    return jnp.dot(a, b, preferred_element_type=jnp.float32)


def step_kernel(
    chips,
    cap,
    pieces,
    halo,
    value_ref,
    gate_ref,
    taps_ref,
    gain_ref,
    wo_hbm,
    rows_ref,
    egain_ref,
    routes_t_ref,
    rw_t_ref,
    wg_hbm,
    wu_hbm,
    wd_hbm,
    mixer_ref,
    routed_ref,
    wo,
    wg,
    wu,
    wd,
    normed,
    picked,
    block,
    hid,
    part,
    pair_in,
    cross_out,
    cross_in,
    back_out,
    results,
    glu,
    halo_in,
    conv,
    w_sem,
    disp_send,
    disp_recv,
    xf_send,
    xf_recv,
    cf_send,
    cf_recv,
    r1_send,
    r1_recv,
    r2_send,
    r2_recv,
    r3_send,
    r3_recv,
    ag_send,
    ag_recv,
    halo_send,
    halo_recv,
):
    f32, bf16 = jnp.float32, jnp.bfloat16
    ep = lax.axis_index("ep")
    x = lax.axis_index("tp")
    n_ep = 2 * chips
    z, c = lax.div(ep, 2), lax.rem(ep, 2)
    width = block.shape[-1]
    tokens = rows_ref.shape[0]
    length, local = value_ref.shape
    cols = local // LANES
    ntaps = taps_ref.shape[0]
    split_from = max(1, chips // 2)
    peers = [_xor(z, k) for k in range(chips)]

    def dev(zd, cd, xd):
        return {"ep": zd * 2 + cd, "tp": xd}

    def remote(src, dst, send, recv, to):
        return pltpu.make_async_remote_copy(
            src_ref=src, dst_ref=dst, send_sem=send, recv_sem=recv, device_id=to, device_id_type=MESH
        )

    core_peer = dev(z, 1 - c, x)
    plane_peer = dev(z, c, 1 - x)
    after = {"ep": lax.rem(ep + 1, n_ep), "tp": x}
    prior = {"ep": lax.rem(ep + n_ep - 1, n_ep), "tp": x}

    weights = [
        pltpu.make_async_copy(wg_hbm.at[0], wg, w_sem.at[0]),
        pltpu.make_async_copy(wu_hbm.at[0], wu, w_sem.at[1]),
        pltpu.make_async_copy(wd_hbm.at[0], wd, w_sem.at[2]),
        pltpu.make_async_copy(wo_hbm, wo, w_sem.at[3]),
    ]
    for copy in weights:
        copy.start()

    barrier = pltpu.get_barrier_semaphore()
    greeted = [core_peer, plane_peer, after, prior] + [dev(peers[k], c, x) for k in range(1, chips)]
    for to in greeted:
        pl.semaphore_signal(barrier, inc=1, device_id=to, device_id_type=MESH)

    erows = -(-chips // 8) * 8
    r0t, r1t = routes_t_ref[0:1, :], routes_t_ref[1:2, :]
    eid = _iota((erows, tokens), 0)
    hits_t = (r0t == eid) | (r1t == eid)
    earlier_t = (_iota((tokens, tokens), 0) < _iota((tokens, tokens), 1)).astype(f32)
    place_t = _dot(hits_t.astype(f32).astype(bf16), earlier_t.astype(bf16))
    slot_t = jnp.where(hits_t, place_t, -1.0).astype(jnp.int32)

    rows = rows_ref[...].astype(f32)
    scale = lax.rsqrt(jnp.mean(rows * rows, axis=-1, keepdims=True) + eps)
    both = (rows * scale * egain_ref[...]).astype(bf16)
    normed[0] = both[:, :width]
    normed[1] = both[:, width:]

    sends = []
    slots = _iota((cap, tokens), 0)

    def pick(k):
        row = jnp.sum(jnp.where(eid == peers[k], slot_t, 0), axis=0, keepdims=True)
        return (slots == row).astype(f32).astype(bf16)

    for k in range(chips - 1, 0, -1):
        picker = pick(k)
        if k >= split_from:
            picked[k, 0] = _dot(picker, normed[x]).astype(bf16)
        else:
            for h in range(2):
                picked[k, h] = _dot(picker, normed[h]).astype(bf16)
    picker = pick(0)
    for h in range(2):
        block[z, h, c] = _dot(picker, normed[h]).astype(bf16)

    pl.semaphore_wait(barrier, len(greeted))
    subs = 2 if cap % 32 == 0 else 1
    far = list(range(split_from, chips))
    near = list(range(1, split_from))

    def sub(s):
        return pl.ds(s * (cap // subs), cap // subs)

    for k in far + near:
        to = dev(peers[k], c, x)
        if k >= split_from:
            copies = [
                remote(
                    picked.at[k, 0, sub(s)],
                    block.at[z, x, c, sub(s)],
                    disp_send.at[k, s],
                    disp_recv.at[z, s],
                    to,
                )
                for s in range(subs)
            ]
        else:
            copies = [
                remote(
                    picked.at[k, h], block.at[z, h, c], disp_send.at[k, h], disp_recv.at[z, h], to
                )
                for h in range(2)
            ]
        for copy in copies:
            copy.start()
        sends.extend(copies)

    def start(copy):
        copy.start()
        sends.append(copy)

    whole = pl.ds(0, cap)

    def to_core(k, h, sem, rows_of=whole):
        here = block.at[peers[k], h, c, rows_of]
        start(remote(here, here, cf_send.at[k, sem], cf_recv.at[k, sem], core_peer))

    def from_core(k, h, sem, rows_of=whole):
        here = block.at[peers[k], h, 1 - c, rows_of]
        remote(here, here, cf_send.at[k, sem], cf_recv.at[k, sem], core_peer).wait_recv()

    def arrived(k, h, sem, rows_of=whole):
        here = block.at[peers[k], h, c, rows_of]
        remote(
            here, here, disp_send.at[k, sem], disp_recv.at[peers[k], sem], dev(peers[k], c, x)
        ).wait_recv()

    def experts(k):
        zs = peers[k]
        a0 = block[zs, 0].reshape(2 * cap, width)
        a1 = block[zs, 1].reshape(2 * cap, width)
        units = hid.shape[1]
        step = min(units, 256)
        for j in range(0, units, step):
            gate = _dot(a0, wg[:width, j : j + step]) + _dot(a1, wg[width:, j : j + step])
            up = _dot(a0, wu[:width, j : j + step]) + _dot(a1, wu[width:, j : j + step])
            hid[:, j : j + step] = (gate * jax.nn.sigmoid(gate) * up).astype(bf16)
        h_all = hid[...]
        for h in range(2):
            for j in range(0, width, step):
                out = _dot(h_all, wd[:, h * width + j : h * width + j + step]).astype(bf16)
                part[k, 0, h, :, j : j + step] = out[:cap]
                part[k, 1, h, :, j : j + step] = out[cap:]
        start(remote(part.at[k, 1 - c], pair_in.at[k], r1_send.at[k], r1_recv.at[k], core_peer))

    def pair_sum(k):
        remote(
            part.at[k, 1 - c], pair_in.at[k], r1_send.at[k], r1_recv.at[k], core_peer
        ).wait_recv()
        total = part[k, c, 1 - x].astype(f32) + pair_in[k, 1 - x].astype(f32)
        cross_out[k] = total.astype(bf16)
        start(remote(cross_out.at[k], cross_in.at[k], r2_send.at[k], r2_recv.at[k], plane_peer))

    def plane_sum(k):
        remote(
            cross_out.at[k], cross_in.at[k], r2_send.at[k], r2_recv.at[k], plane_peer
        ).wait_recv()
        total = part[k, c, x].astype(f32) + pair_in[k, x].astype(f32) + cross_in[k].astype(f32)
        if k == 0:
            results[z] = total.astype(bf16)
        else:
            back_out[k] = total.astype(bf16)
            start(
                remote(
                    back_out.at[k],
                    results.at[z],
                    r3_send.at[k],
                    r3_recv.at[z],
                    dev(peers[k], c, x),
                )
            )

    for h in range(2):
        to_core(0, h, h)

    for i in range(cols):
        part_cols = slice(i * LANES, (i + 1) * LANES)
        gated = value_ref[:, part_cols].astype(f32) * jax.nn.sigmoid(
            gate_ref[:, part_cols].astype(f32)
        )
        glu[i, halo:, :] = gated.astype(bf16).astype(f32)
    start(
        remote(
            glu.at[:, pl.ds(length, halo)], halo_in, halo_send.at[0], halo_recv.at[0], after
        )
    )

    for h in range(2):
        from_core(0, h, h)
    for copy in weights[:3]:
        copy.wait()
    experts(0)

    remote(
        glu.at[:, pl.ds(length, halo)], halo_in, halo_send.at[0], halo_recv.at[0], after
    ).wait_recv()
    glu[:, :halo, :] = jnp.where(ep > 0, halo_in[...], 0.0)
    tile = 64 if length % 64 == 0 else length
    for i in range(cols):

        def conv_tile(r, carry):
            r0 = pl.multiple_of(r * tile, tile)
            total = jnp.zeros((tile, LANES), f32)
            for k in range(ntaps):
                total = (
                    total
                    + taps_ref[k : k + 1, i * LANES : (i + 1) * LANES]
                    * glu[i, pl.ds(r0 + (k + halo - ntaps + 1), tile), :]
                )
            conv[x, pl.ds(r0, tile), i * LANES : (i + 1) * LANES] = total.astype(bf16)
            return carry

        lax.fori_loop(0, length // tile, conv_tile, 0)

    rows_per = length // pieces

    def gather_copy(p):
        own = conv.at[x, pl.ds(p * rows_per, rows_per)]
        return remote(own, own, ag_send.at[p], ag_recv.at[p], plane_peer)

    def gather_some(lo, hi):
        for p in range(lo, hi):
            start(gather_copy(p))

    gather_some(0, 1)
    for k in far:
        for s in range(subs):
            arrived(k, x, s, sub(s))
            here = block.at[peers[k], x, c, sub(s)]
            start(remote(here, here, xf_send.at[k, s], xf_recv.at[k, s], plane_peer))
            to_core(k, x, s, sub(s))
    pair_sum(0)
    for k in near:
        for h in range(2):
            arrived(k, h, h)
            to_core(k, h, h)
    for k in near:
        for h in range(2):
            from_core(k, h, h)
        experts(k)
    for k in far:
        for s in range(subs):
            here = block.at[peers[k], 1 - x, c, sub(s)]
            remote(here, here, xf_send.at[k, s], xf_recv.at[k, s], plane_peer).wait_recv()
            to_core(k, 1 - x, subs + s, sub(s))
        if k == far[0]:
            for q in near:
                pair_sum(q)
        for s in range(subs):
            from_core(k, x, s, sub(s))
            from_core(k, 1 - x, subs + s, sub(s))
        experts(k)
        if k > far[0]:
            plane_sum(k - 1)
        pair_sum(k)
    gather_some(1, pieces)
    for k in near:
        plane_sum(k)
    plane_sum(chips - 1)
    plane_sum(0)

    weights[3].wait()
    for p in range(pieces):
        other = conv.at[1 - x, pl.ds(p * rows_per, rows_per)]
        remote(other, other, ag_send.at[p], ag_recv.at[p], plane_peer).wait_recv()
        here = slice(p * rows_per, (p + 1) * rows_per)
        lo, hi = conv[0, here, :].astype(f32), conv[1, here, :].astype(f32)
        count = 2 * local
        mean = (
            jnp.sum(lo, axis=-1, keepdims=True) + jnp.sum(hi, axis=-1, keepdims=True)
        ) / count
        lo, hi = lo - mean, hi - mean
        var = (
            jnp.sum(lo * lo, axis=-1, keepdims=True) + jnp.sum(hi * hi, axis=-1, keepdims=True)
        ) / count
        scale = lax.rsqrt(var + eps)
        lo = lo * scale * gain_ref[:, :local]
        hi = hi * scale * gain_ref[:, local:]
        lo = (lo * jax.nn.sigmoid(lo)).astype(bf16)
        hi = (hi * jax.nn.sigmoid(hi)).astype(bf16)
        mixer_ref[here, :] = (_dot(lo, wo[:local, :]) + _dot(hi, wo[local:, :])).astype(bf16)

    lane = _iota((tokens, LANES), 1)
    index = _iota((8, tokens), 0)
    rows_named = jnp.where(index == 0, r0t, 0).astype(f32) + jnp.where(index == 1, r1t, 0).astype(f32)
    for j in range(2):
        rows_named = rows_named + jnp.where(index == 2 + j, rw_t_ref[j : j + 1, :], 0.0)
    named = jnp.transpose(rows_named)
    r0, r1 = (named[:, j : j + 1].astype(jnp.int32) for j in range(2))
    hits = ((r0 == lane) | (r1 == lane)).astype(f32).astype(bf16)
    earlier = (_iota((tokens, tokens), 1) < _iota((tokens, tokens), 0)).astype(f32).astype(bf16)
    place = _dot(earlier, hits)
    all_slots = _iota((tokens, chips * cap), 1)
    comb = jnp.zeros((tokens, chips * cap), f32)
    for j, r in enumerate((r0, r1)):
        at = jnp.sum(jnp.where(lane == r, place, 0.0), axis=1, keepdims=True).astype(jnp.int32)
        comb = comb + jnp.where(all_slots == r * cap + at, named[:, 2 + j : 3 + j], 0.0)
    head = comb.astype(bf16)
    tail = (comb - head.astype(f32)).astype(bf16)
    for k in range(1, chips):
        zs = peers[k]
        remote(
            back_out.at[k], results.at[zs], r3_send.at[k], r3_recv.at[zs], dev(zs, c, x)
        ).wait_recv()
    found = results[...].reshape(chips * cap, width)
    routed_ref[...] = (_dot(head, found) + _dot(tail, found)).astype(bf16)
    for copy in sends:
        copy.wait_send()


def one_kernel(
    value_in,
    gate_in,
    conv_taps,
    chan_gain,
    out_weight,
    second_rows,
    expert_gain,
    routes,
    route_weights,
    gate_w,
    up_w,
    down_w,
):
    chips = lax.axis_size("ep") // 2
    tokens, model = second_rows.shape
    top = routes.shape[1]
    width = model // 2
    cap = 2 * max(1, min(tokens // 2, 3 * tokens * top // (4 * chips)))
    length, local = value_in.shape
    units = gate_w.shape[2]
    halo = -(-(conv_taps.shape[0] - 1) // 8) * 8
    pieces = 4
    bf16, f32 = jnp.bfloat16, jnp.float32
    vmem = pl.BlockSpec(memory_space=pltpu.VMEM)
    hbm = pl.BlockSpec(memory_space=pl.ANY)
    dma = pltpu.SemaphoreType.DMA
    scratch = [
        pltpu.VMEM(out_weight.shape, bf16),
        pltpu.VMEM(gate_w.shape[1:], bf16),
        pltpu.VMEM(up_w.shape[1:], bf16),
        pltpu.VMEM(down_w.shape[1:], bf16),
        pltpu.VMEM((2, tokens, width), bf16),
        pltpu.VMEM((chips, 2, cap, width), bf16),
        pltpu.VMEM((chips, 2, 2, cap, width), bf16),
        pltpu.VMEM((2 * cap, units), bf16),
        pltpu.VMEM((chips, 2, 2, cap, width), bf16),
        pltpu.VMEM((chips, 2, cap, width), bf16),
        pltpu.VMEM((chips, cap, width), bf16),
        pltpu.VMEM((chips, cap, width), bf16),
        pltpu.VMEM((chips, cap, width), bf16),
        pltpu.VMEM((chips, cap, width), bf16),
        pltpu.VMEM((local // LANES, halo + length, LANES), f32),
        pltpu.VMEM((local // LANES, halo, LANES), f32),
        pltpu.VMEM((2, length, local), bf16),
        dma((4,)),
        dma((chips, 2)),
        dma((chips, 2)),
        dma((chips, 2)),
        dma((chips, 2)),
        dma((chips, 4)),
        dma((chips, 4)),
        dma((chips,)),
        dma((chips,)),
        dma((chips,)),
        dma((chips,)),
        dma((chips,)),
        dma((chips,)),
        dma((pieces,)),
        dma((pieces,)),
        dma((1,)),
        dma((1,)),
    ]
    return pl.pallas_call(
        functools.partial(step_kernel, chips, cap, pieces, halo),
        out_shape=(
            jax.ShapeDtypeStruct((length, out_weight.shape[1]), bf16),
            jax.ShapeDtypeStruct((tokens, width), bf16),
        ),
        in_specs=[vmem] * 4 + [hbm] + [vmem] * 4 + [hbm] * 3,
        out_specs=(vmem, vmem),
        scratch_shapes=scratch,
        compiler_params=pltpu.CompilerParams(
            collective_id=0, has_side_effects=True, vmem_limit_bytes=60 * 1024 * 1024
        ),
    )(
        value_in,
        gate_in,
        conv_taps,
        chan_gain.reshape(1, -1),
        out_weight,
        second_rows,
        expert_gain.reshape(1, -1),
        routes.T,
        route_weights.T,
        gate_w,
        up_w,
        down_w,
    )


def solution(mesh):
    chips = mesh.shape["ep"] // 2
    paired = mesh.shape["tp"] == 2 and chips > 1 and chips & (chips - 1) == 0
    placed = (
        P(("grp", "ep"), "tp"),
        P(("grp", "ep"), "tp"),
        P(None, "tp"),
        P(),
        P(None, "tp"),
        P(("grp", "ep"), None),
        P(),
        P(("grp", "ep"), None),
        P(("grp", "ep"), None),
        P("ep", None, "tp"),
        P("ep", None, "tp"),
        P("ep", "tp", None),
    )
    return jax.shard_map(
        one_kernel if paired else on_device,
        mesh=mesh,
        in_specs=placed,
        out_specs=(P(("grp", "ep"), "tp"), P(("grp", "ep"), "tp")),
        check_vma=False,
    )
```

profile of v0, /device:TPU:8, one launch (start us, length us, event | category | flops | bytes accessed | tf_op | source)
XLA Modules:
  0.0 68.9 jit_solution(18412623000148464109)
XLA Ops:
  0.6 64.3 %shard_map.131 = (bf16[512,1024]{1,0:T(8,128)(2,1)}, bf16[128,1024]{1,0:T(8,128)(2,1)}) custom-call(bf16[512,512]{1,0:T(8,128)(2,1)} %value_ref.1, bf16[512,512]{1,0:T(8,128)(2,1)} %gate_ref.1, f32[31,512]{1,0:T(8,128)} %taps_ref.1, f32[1,1024]{1,0:T(1,128)} %bitcast.5, bf16[1024,1024]{1,0:T(8,128)(2,1)} %wo_hbm.1, bf16[128,2048]{1,0:T(8,128)(2,1)} %rows_ref.1, ...), custom_call_target="tpu_custom_call" | custom-call | tf_op jit(solution)/shard_map/pallas_call | solution.py:560
  64.9 2.3 %copy.16 = bf16[512,1024]{1,0:T(8,128)(2,1)} copy(bf16[512,1024]{1,0:T(8,128)(2,1)} %get-tuple-element.4) | data formatting | bytes 2097152
  67.2 1.7 %copy.17 = bf16[128,1024]{1,0:T(8,128)(2,1)} copy(bf16[128,1024]{1,0:T(8,128)(2,1)} %get-tuple-element.5) | data formatting | bytes 524288
where the time goes:
time: 69.1 us; the launch traced here: 68.9 us
  Pallas kernels  64.3 us (93%)
  local copies, waits for them, and re-layouts  3.93 us (6%)
    pallas_call x1, Pallas kernels, one_kernel(): pl.pallas_call(functools.partial(step_kernel, chips, cap, pieces, halo),...  64.3 us
    unnamed x2, local copies, waits for them, and re-layouts  3.93 us

commit v1 on v0

v1 whole, which is shorter than its diff:
```python
import functools

import jax
import jax.numpy as jnp
from jax import lax
from jax.experimental import pallas as pl
from jax.experimental.pallas import tpu as pltpu
from jax.sharding import PartitionSpec as P

eps = 1e-06
LANES = 128
MESH = pl.DeviceIdType.MESH


def partner_2(value, axis, bit):
    return lax.ppermute(value, axis, [(i, i ^ 1 << bit) for i in range(lax.axis_size(axis))])


def shifted(value, axis, by):
    devices = lax.axis_size(axis)
    pairs = [(i, i + by) for i in range(devices) if 0 <= i + by < devices]
    return lax.ppermute(value, axis, pairs)


def partner(block):
    return partner_2(block, "ep", 0)


def across(block):
    return lax.all_to_all(block, "ep", split_axis=0, concat_axis=0, tiled=True)


def on_device(
    value_in,
    gate_in,
    conv_taps,
    chan_gain,
    out_weight,
    second_rows,
    expert_gain,
    routes,
    route_weights,
    gate_w,
    up_w,
    down_w,
):
    taps = conv_taps.shape[0]
    glu = (value_in.astype(jnp.float32) * jax.nn.sigmoid(gate_in.astype(jnp.float32))).astype(
        jnp.bfloat16
    )
    length = glu.shape[0]
    before = shifted(glu[length - taps + 1 :], "ep", 1)
    padded = jnp.concatenate([before, glu], axis=0).astype(jnp.float32)
    total = jnp.zeros(glu.shape, jnp.float32)
    for offset in range(taps):
        total = total + conv_taps[offset][None, :] * padded[offset : offset + length]
    convolved = total.astype(jnp.bfloat16)
    channels = lax.all_gather(convolved, "tp", axis=1, tiled=True)
    values = channels.astype(jnp.float32)
    centered = values - jnp.mean(values, axis=-1, keepdims=True)
    scaled = (
        centered
        * lax.rsqrt(jnp.mean(centered * centered, axis=-1, keepdims=True) + eps)
        * chan_gain
    )
    activated = jax.nn.silu(scaled).astype(jnp.bfloat16)
    mixer_rows = jnp.dot(activated, out_weight, preferred_element_type=jnp.float32).astype(
        jnp.bfloat16
    )
    n_ep = lax.axis_size("ep")
    experts = n_ep // 2
    tokens = second_rows.shape[0]
    top = routes.shape[1]
    width = second_rows.shape[1]
    capacity = 2 * max(1, min(tokens // 2, 3 * tokens * top // (4 * experts)))
    half_slots = capacity // 2
    rows = second_rows.astype(jnp.float32)
    normed = (
        rows * lax.rsqrt(jnp.mean(rows * rows, axis=-1, keepdims=True) + eps) * expert_gain
    ).astype(jnp.bfloat16)
    chosen = routes.reshape(-1)
    hits = (chosen[:, None] == jnp.arange(experts, dtype=jnp.int32)[None, :]).astype(jnp.int32)
    place = jnp.sum((jnp.cumsum(hits, axis=0) - 1) * hits, axis=1)
    target = (chosen * capacity + place).reshape(tokens, top)
    slots = jnp.arange(experts * capacity, dtype=jnp.int32)
    matches = target[:, :, None] == slots[None, None, :]
    picker = jnp.any(matches, axis=1).astype(jnp.bfloat16)
    outgoing = jnp.dot(picker.T, normed, preferred_element_type=jnp.float32).astype(jnp.bfloat16)
    combiner = jnp.sum(jnp.where(matches, route_weights[:, :, None], 0.0), axis=1)
    upper = lax.axis_index("ep") % 2
    arrived = across(outgoing.reshape(n_ep, half_slots, width))
    other = partner(arrived)
    first = jnp.where(upper == 0, arrived, other)
    second = jnp.where(upper == 0, other, arrived)
    incoming = jnp.concatenate([first, second], axis=1)
    block_rows = incoming.reshape(n_ep * capacity, width)
    gate = jnp.dot(block_rows, gate_w[0], preferred_element_type=jnp.float32)
    lifted = jnp.dot(block_rows, up_w[0], preferred_element_type=jnp.float32)
    hidden = (jax.nn.silu(gate) * lifted).astype(jnp.bfloat16)
    partial_value = jnp.dot(hidden, down_w[0], preferred_element_type=jnp.float32)
    half_sums = lax.psum_scatter(
        partial_value.astype(jnp.bfloat16), "tp", scatter_dimension=1, tiled=True
    )
    columns = half_sums.shape[1]
    half_sums = half_sums.reshape(n_ep, capacity, columns)
    other_sums = partner(half_sums)
    joined = (half_sums.astype(jnp.float32) + other_sums.astype(jnp.float32)).astype(jnp.bfloat16)
    own = lax.dynamic_slice_in_dim(joined, upper * half_slots, half_slots, 1)
    results = across(own).reshape(experts * capacity, columns)
    routed_rows = jnp.dot(
        combiner,
        results.astype(jnp.float32),
        precision=lax.Precision.HIGHEST,
        preferred_element_type=jnp.float32,
    ).astype(jnp.bfloat16)
    return (mixer_rows, routed_rows)


def _xor(value, mask):
    out, bit = value, 1
    while bit <= mask:
        if mask & bit:
            out = out + bit - 2 * bit * lax.rem(lax.div(value, bit), 2)
        bit *= 2
    return out


def _iota(shape, dim):
    return lax.broadcasted_iota(jnp.int32, shape, dim)


def _dot(a, b):
    return jnp.dot(a, b, preferred_element_type=jnp.float32)


def step_kernel(
    chips,
    cap,
    subs,
    pieces,
    halo,
    value_hbm,
    gate_hbm,
    taps_hbm,
    gain_hbm,
    wo_hbm,
    rows_hbm,
    egain_hbm,
    routes_hbm,
    rw_hbm,
    wg_hbm,
    wu_hbm,
    wd_hbm,
    mixer_ref,
    routed_ref,
    value_ref,
    gate_ref,
    taps_ref,
    gain_ref,
    rows_ref,
    egain_ref,
    routes_t_ref,
    rw_t_ref,
    wo,
    wg,
    wu,
    wd,
    normed,
    picked,
    block,
    hid,
    part,
    pair_in,
    cross_out,
    cross_in,
    back_out,
    results,
    near_out,
    near_res,
    q_out,
    q_in,
    combs,
    acc,
    glu,
    halo_out,
    halo_in,
    conv,
    w_sem,
    in_sem,
    disp_send,
    disp_recv,
    xf_send,
    xf_recv,
    cf_send,
    cf_recv,
    r1_send,
    r1_recv,
    r2_send,
    r2_recv,
    r3_send,
    r3_recv,
    r4_send,
    r4_recv,
    q_send,
    q_recv,
    ag_send,
    ag_recv,
    halo_send,
    halo_recv,
):
    f32, bf16 = jnp.float32, jnp.bfloat16
    ep = lax.axis_index("ep")
    x = lax.axis_index("tp")
    n_ep = 2 * chips
    z, c = lax.div(ep, 2), lax.rem(ep, 2)
    width = block.shape[-1]
    tokens = rows_ref.shape[0]
    length, local = value_ref.shape
    cols = local // LANES
    ntaps = taps_ref.shape[0]
    few = cap // subs
    split_from = max(1, chips // 2)
    far = list(range(split_from, chips))
    near = list(range(1, split_from))
    swap = 1 - lax.rem(z + lax.div(z, 2), 2)
    peers = [_xor(z, k) for k in range(chips)]
    for k in far:
        peers[k] = peers[k] + swap * (1 - 2 * lax.rem(peers[k], 2))

    def dev(zd, cd, xd):
        return {"ep": zd * 2 + cd, "tp": xd}

    def remote(src, dst, send, recv, to):
        return pltpu.make_async_remote_copy(
            src_ref=src, dst_ref=dst, send_sem=send, recv_sem=recv, device_id=to, device_id_type=MESH
        )

    core_peer = dev(z, 1 - c, x)
    plane_peer = dev(z, c, 1 - x)
    after = {"ep": lax.rem(ep + 1, n_ep), "tp": x}
    prior = {"ep": lax.rem(ep + n_ep - 1, n_ep), "tp": x}
    sends = []

    def start(copy):
        copy.start()
        sends.append(copy)

    barrier = pltpu.get_barrier_semaphore()
    greeted = [core_peer, plane_peer, after, prior] + [dev(peers[k], c, x) for k in range(1, chips)]
    for to in greeted:
        pl.semaphore_signal(barrier, inc=1, device_id=to, device_id_type=MESH)

    inputs = [
        (rows_hbm, rows_ref),
        (routes_hbm, routes_t_ref),
        (rw_hbm, rw_t_ref),
        (egain_hbm, egain_ref),
        (value_hbm, value_ref),
        (gate_hbm, gate_ref),
        (taps_hbm, taps_ref),
        (gain_hbm, gain_ref),
    ]
    inputs = [pltpu.make_async_copy(a, b, in_sem.at[i]) for i, (a, b) in enumerate(inputs)]
    weights = [
        pltpu.make_async_copy(wg_hbm.at[0], wg, w_sem.at[0]),
        pltpu.make_async_copy(wu_hbm.at[0], wu, w_sem.at[1]),
        pltpu.make_async_copy(wd_hbm.at[0], wd, w_sem.at[2]),
        pltpu.make_async_copy(wo_hbm, wo, w_sem.at[3]),
    ]
    for copy in inputs:
        copy.start()
    for copy in inputs[:4]:
        copy.wait()
    erows = -(-chips // 8) * 8
    r0t, r1t = routes_t_ref[0:1, :], routes_t_ref[1:2, :]
    eid = _iota((erows, tokens), 0)
    hits_t = (r0t == eid) | (r1t == eid)
    earlier_t = (_iota((tokens, tokens), 0) < _iota((tokens, tokens), 1)).astype(f32)
    place_t = _dot(hits_t.astype(f32).astype(bf16), earlier_t.astype(bf16))
    slot_t = jnp.where(hits_t, place_t, -1.0).astype(jnp.int32)

    rows = rows_ref[...].astype(f32)
    scale = lax.rsqrt(jnp.mean(rows * rows, axis=-1, keepdims=True) + eps)
    both = (rows * scale * egain_ref[...]).astype(bf16)
    normed[0] = both[:, :width]
    normed[1] = both[:, width:]

    slots = _iota((cap, tokens), 0)

    def pick(k):
        row = jnp.sum(jnp.where(eid == peers[k], slot_t, 0), axis=0, keepdims=True)
        return (slots == row).astype(f32).astype(bf16)

    def cut(s):
        return slice(s * few, (s + 1) * few)

    for k in far:
        rows_k = _dot(pick(k), normed[x]).astype(bf16)
        for s in range(subs):
            picked[k, 0, s] = rows_k[cut(s)]
    for copy in inputs[4:]:
        copy.wait()
    for copy in weights:
        copy.start()
    last = slice(length - halo, length)
    gated = value_ref[last, :].astype(f32) * jax.nn.sigmoid(gate_ref[last, :].astype(f32))
    halo_out[...] = gated.astype(bf16)

    pl.semaphore_wait(barrier, len(greeted))
    halo_copy = remote(halo_out, halo_in, halo_send.at[0], halo_recv.at[0], after)
    start(halo_copy)

    def dispatch(k, h, s, slot):
        start(
            remote(
                picked.at[k, slot, s],
                block.at[z, h, s, c],
                disp_send.at[k, slot, s],
                disp_recv.at[z, slot, s],
                dev(peers[k], c, x),
            )
        )

    def arrived(k, h, s, slot):
        here = block.at[peers[k], h, s, c]
        remote(
            here, here, disp_send.at[k, slot, s], disp_recv.at[peers[k], slot, s], dev(peers[k], c, x)
        ).wait_recv()

    def to_core(k, h, s):
        here = block.at[peers[k], h, s, c]
        start(remote(here, here, cf_send.at[k, h, s], cf_recv.at[k, h, s], core_peer))

    def from_core(k, h, s):
        here = block.at[peers[k], h, s, 1 - c]
        remote(here, here, cf_send.at[k, h, s], cf_recv.at[k, h, s], core_peer).wait_recv()

    def plane_copy(k, h, s):
        here = block.at[peers[k], h, s, c]
        return remote(here, here, xf_send.at[k, s], xf_recv.at[k, s], plane_peer)

    def pair_copy(k, o, s, n):
        h = x if o else 1 - x
        span = pl.ds(s * few, n)
        return remote(
            part.at[k, 1 - c, h, span],
            pair_in.at[k, h, span],
            r1_send.at[k, o, s],
            r1_recv.at[k, o, s],
            core_peer,
        )

    def cross_copy(k, s, n):
        span = pl.ds(s * few, n)
        return remote(
            cross_out.at[k, span], cross_in.at[k, span], r2_send.at[k, s], r2_recv.at[k, s], plane_peer
        )

    def back_copy(k, s, n, at):
        span = pl.ds(s * few, n)
        return remote(
            back_out.at[k, span],
            results.at[at, span],
            r3_send.at[k, s],
            r3_recv.at[at, s],
            dev(peers[k], c, x),
        )

    def feed_forward(k, s, n, between=None, after_half=None):
        count = n // few
        zs = peers[k]
        a0 = block[zs, 0, s : s + count].reshape(2 * n, width)
        a1 = block[zs, 1, s : s + count].reshape(2 * n, width)
        units = hid.shape[1]
        step = min(units, 256)
        for j in range(0, units, step):
            gate = _dot(a0, wg[:width, j : j + step]) + _dot(a1, wg[width:, j : j + step])
            up = _dot(a0, wu[:width, j : j + step]) + _dot(a1, wu[width:, j : j + step])
            hid[: 2 * n, j : j + step] = (gate * jax.nn.sigmoid(gate) * up).astype(bf16)
        if between:
            between()
        h_all = hid[: 2 * n, :]
        for o in range(2):
            if o and after_half:
                after_half()
            h = x if o else 1 - x
            for j in range(0, width, step):
                at = pl.ds(pl.multiple_of(h * width + j, step), step)
                out = _dot(h_all, wd[:, at]).astype(bf16)
                for i in range(count):
                    for core in range(2):
                        r = (2 * i + core) * few
                        part[k, core, h, cut(s + i), j : j + step] = out[r : r + few]
            start(pair_copy(k, o, s, n))

    def pair_sum(k, s, n, wait=True):
        if wait:
            pair_copy(k, 0, s, n).wait_recv()
        span = slice(s * few, s * few + n)
        total = part[k, c, 1 - x, span].astype(f32) + pair_in[k, 1 - x, span].astype(f32)
        cross_out[k, span] = total.astype(bf16)
        start(cross_copy(k, s, n))

    def plane_sum(k, s, n, wait=True):
        if wait:
            pair_copy(k, 1, s, n).wait_recv()
        cross_copy(k, s, n).wait_recv()
        span = slice(s * few, s * few + n)
        total = (
            part[k, c, x, span].astype(f32)
            + pair_in[k, x, span].astype(f32)
            + cross_in[k, span].astype(f32)
        )
        back_out[k, span] = total.astype(bf16)
        start(back_copy(k, s, n, z))

    def near_copy(k, o):
        return remote(
            near_out.at[k, o], near_res.at[k, o], r4_send.at[k, o], r4_recv.at[k, o], dev(peers[k], c, x)
        )

    def near_sum(k, o):
        pair_copy(k, o, 0, cap).wait_recv()
        h = x if o else 1 - x
        total = part[k, c, h].astype(f32) + pair_in[k, h].astype(f32)
        near_out[k, o] = total.astype(bf16)
        if k:
            start(near_copy(k, o))

    q_copy = remote(q_out, q_in, q_send.at[0], q_recv.at[0], plane_peer)

    def close(o):
        total = weighed(0, near_out[0, o])
        for k in near:
            near_copy(k, o).wait_recv()
            total = total + weighed(k, near_res[k, o])
        if o:
            acc[...] = total
        else:
            q_out[...] = total.astype(bf16)
            start(q_copy)

    def pair_sums(k):
        pair_copy(k, 0, 0, cap).wait_recv()
        for s in range(subs):
            pair_sum(k, s, few, False)

    def plane_sums(k):
        pair_copy(k, 1, 0, cap).wait_recv()
        for s in range(subs):
            plane_sum(k, s, few, False)

    def send_far():
        for s in range(subs):
            for k in far:
                dispatch(k, x, s, 0)

    def far_in(k, s):
        arrived(k, x, s, 0)
        start(plane_copy(k, x, s))
        to_core(k, x, s)

    def far_over(k, s):
        plane_copy(k, 1 - x, s).wait_recv()
        to_core(k, 1 - x, s)

    def far_experts(k, s):
        for h in range(2):
            from_core(k, h, s)
        feed_forward(k, s, few)

    def near_in(k):
        for h in range(2):
            for s in range(subs):
                arrived(k, h, s, h)
                to_core(k, h, s)

    def from_cores(k):
        for h in range(2):
            for s in range(subs):
                from_core(k, h, s)

    def weighed(k, found):
        return _dot(combs[k, 0], found) + _dot(combs[k, 1], found)

    rows_per = length // pieces
    tile = 64 if rows_per % 64 == 0 else rows_per

    def gather_copy(p, who):
        rows_p = conv.at[who, pl.ds(p * rows_per, rows_per)]
        return remote(rows_p, rows_p, ag_send.at[p], ag_recv.at[p], plane_peer)

    def gather(lo, hi):
        for p in range(lo, hi):
            start(gather_copy(p, x))

    def convolve(lo, hi, send=False):
        def conv_tile(r, carry):
            r0 = pl.multiple_of(r * tile, tile)
            for i in range(cols):
                total = jnp.zeros((tile, LANES), f32)
                for k in range(ntaps):
                    total = (
                        total
                        + taps_ref[k : k + 1, i * LANES : (i + 1) * LANES]
                        * glu[i, pl.ds(r0 + (k + halo - ntaps + 1), tile), :]
                    )
                conv[x, pl.ds(r0, tile), i * LANES : (i + 1) * LANES] = total.astype(bf16)
            if send:
                gather_copy(r, x).start()
            return carry

        per = rows_per // tile
        send = send and per == 1
        lax.fori_loop(lo * per, hi * per, conv_tile, 0)
        if send:
            sends.extend(gather_copy(p, x) for p in range(lo, hi))
        return send

    def mix(lo, hi):
        for p in range(lo, hi):
            gather_copy(p, 1 - x).wait_recv()
        here = slice(lo * rows_per, hi * rows_per)
        first, second = conv[0, here, :].astype(f32), conv[1, here, :].astype(f32)
        count = 2 * local
        mean = (
            jnp.sum(first, axis=-1, keepdims=True) + jnp.sum(second, axis=-1, keepdims=True)
        ) / count
        first, second = first - mean, second - mean
        var = (
            jnp.sum(first * first, axis=-1, keepdims=True)
            + jnp.sum(second * second, axis=-1, keepdims=True)
        ) / count
        scale = lax.rsqrt(var + eps)
        first = first * scale * gain_ref[:, :local]
        second = second * scale * gain_ref[:, local:]
        first = (first * jax.nn.sigmoid(first)).astype(bf16)
        second = (second * jax.nn.sigmoid(second)).astype(bf16)
        mixer_ref[here, :] = (_dot(first, wo[:local, :]) + _dot(second, wo[local:, :])).astype(bf16)

    def combine(k):
        return acc[...] + weighed(k, results[peers[k]])

    def returned(k, n):
        for s in range(0, cap // few, n // few):
            zs = peers[k]
            span = pl.ds(s * few, n)
            remote(
                back_out.at[k, span],
                results.at[zs, span],
                r3_send.at[k, s],
                r3_recv.at[zs, s],
                dev(zs, c, x),
            ).wait_recv()

    send_far()
    for k in near:
        rows_k = [_dot(pick(k), normed[h]).astype(bf16) for h in range(2)]
        for h in range(2):
            for s in range(subs):
                picked[k, h, s] = rows_k[h][cut(s)]
                dispatch(k, h, s, h)
    for h in range(2):
        rows_0 = _dot(pick(0), normed[h]).astype(bf16)
        for s in range(subs):
            block[z, h, s, c] = rows_0[cut(s)]
    for h in range(2):
        for s in range(subs):
            to_core(0, h, s)
    kept = slice(0, length - halo)
    for i in range(cols):
        at = slice(i * LANES, (i + 1) * LANES)
        gated = value_ref[kept, at].astype(f32) * jax.nn.sigmoid(gate_ref[kept, at].astype(f32))
        glu[i, halo:length, :] = gated.astype(bf16).astype(f32)
        glu[i, length:, :] = halo_out[:, at].astype(f32)
    early = min(pieces, 4)
    if not convolve(1, early, True):
        gather(1, early)
    convolve(early, pieces)
    mid_far, last_far = far[:-1], far[-1]
    units = [(k, s) for k in mid_far for s in range(subs)]
    for copy in weights[:3]:
        copy.wait()
    from_cores(0)
    feed_forward(0, 0, cap, lambda: far_in(*units[0]))
    halo_copy.wait_recv()
    before = jnp.where(ep > 0, halo_in[...].astype(f32), 0.0)
    for i in range(cols):
        glu[i, :halo, :] = before[:, i * LANES : (i + 1) * LANES]
    convolve(0, 1)
    lane = _iota((tokens, LANES), 1)
    index = _iota((8, tokens), 0)
    rows_named = jnp.where(index == 0, r0t, 0).astype(f32) + jnp.where(index == 1, r1t, 0).astype(f32)
    for j in range(2):
        rows_named = rows_named + jnp.where(index == 2 + j, rw_t_ref[j : j + 1, :], 0.0)
    named = jnp.transpose(rows_named)
    r0, r1 = (named[:, j : j + 1].astype(jnp.int32) for j in range(2))
    hits = ((r0 == lane) | (r1 == lane)).astype(f32).astype(bf16)
    earlier = (_iota((tokens, tokens), 1) < _iota((tokens, tokens), 0)).astype(f32).astype(bf16)
    place = _dot(earlier, hits)
    slot_of = _iota((tokens, cap), 1)
    places = [
        jnp.sum(jnp.where(lane == r, place, 0.0), axis=1, keepdims=True).astype(jnp.int32)
        for r in (r0, r1)
    ]
    for k in range(chips):
        comb = jnp.zeros((tokens, cap), f32)
        for j, r in enumerate((r0, r1)):
            mine = jnp.where(r == peers[k], places[j], -1)
            comb = comb + jnp.where(slot_of == mine, named[:, 2 + j : 3 + j], 0.0)
        head = comb.astype(bf16)
        combs[k, 0] = head
        combs[k, 1] = (comb - head.astype(f32)).astype(bf16)


    far_over(*units[0])
    for unit in units[1:]:
        far_in(*unit)
    later = min(pieces, early + 2)
    gather(early, later)
    for o in range(2):
        near_sum(0, o)
    for h in range(2):
        from_core(units[0][0], h, units[0][1])
    feed_forward(*units[0], few)
    for i in range(1, len(units)):
        far_over(*units[i])
        pair_sum(*units[i - 1], few)
        for h in range(2):
            from_core(units[i][0], h, units[i][1])
        feed_forward(*units[i], few, (lambda: far_in(last_far, 0)) if i == 1 else None)
    if len(units) == 1:
        far_in(last_far, 0)
    for k in near:
        near_in(k)
    pair_sum(*units[-1], few)
    far_over(last_far, 0)
    for s in range(1, subs):
        far_in(last_far, s)
    gather(later, pieces)
    gather(0, 1)
    for k in near:
        from_cores(k)
    for k in near:
        feed_forward(k, 0, cap, (lambda: plane_sum(*units[0], few)) if k == near[0] else None)
    for k in near:
        near_sum(k, 0)
    for s in range(1, subs):
        far_over(last_far, s)
    for k in near:
        near_sum(k, 1)
    for unit in units[1:]:
        plane_sum(*unit, few)
    from_cores(last_far)
    feed_forward(last_far, 0, cap)
    pair_sums(last_far)
    weights[3].wait()
    group = 2 if pieces % 2 == 0 else 1
    half = pieces // 2 // group * group
    for p in range(group, half, group):
        mix(p, p + group)
    close(0)
    plane_sums(last_far)
    close(1)
    for p in range(max(half, group), pieces, group):
        mix(p, p + group)
    mix(0, group)
    for k in far[:-1]:
        returned(k, few)
        acc[...] = combine(k)
    q_copy.wait_recv()
    acc[...] = acc[...] + q_in[...].astype(f32)
    returned(far[-1], few)
    routed_ref[...] = combine(far[-1]).astype(bf16)

    for copy in sends:
        copy.wait_send()


def one_kernel(
    value_in,
    gate_in,
    conv_taps,
    chan_gain,
    out_weight,
    second_rows,
    expert_gain,
    routes,
    route_weights,
    gate_w,
    up_w,
    down_w,
):
    chips = lax.axis_size("ep") // 2
    tokens, model = second_rows.shape
    top = routes.shape[1]
    width = model // 2
    cap = 2 * max(1, min(tokens // 2, 3 * tokens * top // (4 * chips)))
    subs = 2 if cap % 32 == 0 else 1
    few = cap // subs
    length, local = value_in.shape
    units = gate_w.shape[2]
    halo = -(-(conv_taps.shape[0] - 1) // 16) * 16
    pieces = 8 if length % 128 == 0 and length // 8 > halo else 1
    bf16, f32 = jnp.bfloat16, jnp.float32
    vmem = pl.BlockSpec(memory_space=pltpu.VMEM)
    hbm = pl.BlockSpec(memory_space=pltpu.HBM)
    dma = pltpu.SemaphoreType.DMA
    scratch = [
        pltpu.VMEM(value_in.shape, bf16),
        pltpu.VMEM(gate_in.shape, bf16),
        pltpu.VMEM(conv_taps.shape, f32),
        pltpu.VMEM((1, chan_gain.shape[0]), f32),
        pltpu.VMEM(second_rows.shape, bf16),
        pltpu.VMEM((1, model), f32),
        pltpu.VMEM((top, tokens), jnp.int32),
        pltpu.VMEM((top, tokens), f32),
        pltpu.VMEM(out_weight.shape, bf16),
        pltpu.VMEM(gate_w.shape[1:], bf16),
        pltpu.VMEM(up_w.shape[1:], bf16),
        pltpu.VMEM(down_w.shape[1:], bf16),
        pltpu.VMEM((2, tokens, width), bf16),
        pltpu.VMEM((chips, 2, subs, few, width), bf16),
        pltpu.VMEM((chips, 2, subs, 2, few, width), bf16),
        pltpu.VMEM((2 * cap, units), bf16),
        pltpu.VMEM((chips, 2, 2, cap, width), bf16),
        pltpu.VMEM((chips, 2, cap, width), bf16),
        pltpu.VMEM((chips, cap, width), bf16),
        pltpu.VMEM((chips, cap, width), bf16),
        pltpu.VMEM((chips, cap, width), bf16),
        pltpu.VMEM((chips, cap, width), bf16),
        pltpu.VMEM((chips // 2, 2, cap, width), bf16),
        pltpu.VMEM((chips // 2, 2, cap, width), bf16),
        pltpu.VMEM((tokens, width), bf16),
        pltpu.VMEM((tokens, width), bf16),
        pltpu.VMEM((chips, 2, tokens, cap), bf16),
        pltpu.VMEM((tokens, width), f32),
        pltpu.VMEM((local // LANES, halo + length, LANES), f32),
        pltpu.VMEM((halo, local), bf16),
        pltpu.VMEM((halo, local), bf16),
        pltpu.VMEM((2, length, local), bf16),
        dma((4,)),
        dma((8,)),
        dma((chips, 2, subs)),
        dma((chips, 2, subs)),
        dma((chips, subs)),
        dma((chips, subs)),
        dma((chips, 2, subs)),
        dma((chips, 2, subs)),
        dma((chips, 2, subs)),
        dma((chips, 2, subs)),
        dma((chips, subs)),
        dma((chips, subs)),
        dma((chips, subs)),
        dma((chips, subs)),
        dma((chips // 2, 2)),
        dma((chips // 2, 2)),
        dma((1,)),
        dma((1,)),
        dma((pieces,)),
        dma((pieces,)),
        dma((1,)),
        dma((1,)),
    ]
    return pl.pallas_call(
        functools.partial(step_kernel, chips, cap, subs, pieces, halo),
        out_shape=(
            jax.ShapeDtypeStruct((length, out_weight.shape[1]), bf16),
            jax.ShapeDtypeStruct((tokens, width), bf16),
        ),
        in_specs=[hbm] * 12,
        out_specs=(vmem, vmem),
        scratch_shapes=scratch,
        compiler_params=pltpu.CompilerParams(
            collective_id=0, has_side_effects=True, vmem_limit_bytes=40 * 1024 * 1024
        ),
    )(
        *(
            pltpu.with_memory_space_constraint(value, pltpu.HBM)
            for value in (
                value_in,
                gate_in,
                conv_taps,
                chan_gain.reshape(1, -1),
                out_weight,
                second_rows,
                expert_gain.reshape(1, -1),
                routes.T,
                route_weights.T,
                gate_w,
                up_w,
                down_w,
            )
        )
    )


def solution(mesh):
    chips = mesh.shape["ep"] // 2
    paired = mesh.shape["tp"] == 2 and chips > 1 and chips & (chips - 1) == 0
    placed = (
        P(("grp", "ep"), "tp"),
        P(("grp", "ep"), "tp"),
        P(None, "tp"),
        P(),
        P(None, "tp"),
        P(("grp", "ep"), None),
        P(),
        P(("grp", "ep"), None),
        P(("grp", "ep"), None),
        P("ep", None, "tp"),
        P("ep", None, "tp"),
        P("ep", "tp", None),
    )
    return jax.shard_map(
        one_kernel if paired else on_device,
        mesh=mesh,
        in_specs=placed,
        out_specs=(P(("grp", "ep"), "tp"), P(("grp", "ep"), "tp")),
        check_vma=False,
    )
```

time: 69.1 us -> 54.5 us (0.79)
  Pallas kernels: 64.3 us -> 51.4 us
  local copies, waits for them, and re-layouts: 3.93 us -> 1.67 us
    pallas_call x1, Pallas kernels: 64.3 us -> 51.4 us  [one_kernel(): pl.pallas_call(functools.partial(step_kernel, chips, cap, subs, pieces, h...]
    unnamed x2, local copies, waits for them, and re-layouts: 3.93 us -> 1.67 us
where the time goes in v1:
time: 54.5 us; the launch traced here: 53.7 us
  Pallas kernels  51.4 us (94%)
  local copies, waits for them, and re-layouts  1.67 us (3%)
  between operations  0.64 us (1%)
    pallas_call x1, Pallas kernels, one_kernel(): pl.pallas_call(functools.partial(step_kernel, chips, cap, subs, pieces, h...  51.4 us
    unnamed x2, local copies, waits for them, and re-layouts  1.67 us

profile of v1, /device:TPU:8, one launch (start us, length us, event | category | flops | bytes accessed | tf_op | source)
XLA Modules:
  0.0 53.7 jit_solution(7961475850847785620)
XLA Ops:
  0.6 51.4 %shard_map.131 = (bf16[512,1024]{1,0:T(8,128)(2,1)S(1)}, bf16[128,1024]{1,0:T(8,128)(2,1)S(1)}) custom-call(bf16[512,512]{1,0:T(8,128)(2,1)} %value_hbm.1, bf16[512,512]{1,0:T(8,128)(2,1)} %gate_hbm.1, f32[31,512]{1,0:T(8,128)} %taps_hbm.1, f32[1,1024]{1,0:T(1,128)} %bitcast.5, bf16[1024,1024]{1,0:T(8,128)(2,1)} %wo_hbm.1, bf16[128,2048]{1,0:T(8,128)(2,1)} %rows_hbm.1, ...), custom_call_target="tpu_custom_call" | custom-call | tf_op jit(solution)/shard_map/pallas_call | solution.py:765
  52.1 1.0 %copy.16 = bf16[512,1024]{1,0:T(8,128)(2,1)} copy(bf16[512,1024]{1,0:T(8,128)(2,1)S(1)} %get-tuple-element.4) | data formatting | bytes 2097152
  53.0 0.7 %copy.17 = bf16[128,1024]{1,0:T(8,128)(2,1)} copy(bf16[128,1024]{1,0:T(8,128)(2,1)S(1)} %get-tuple-element.5) | data formatting | bytes 524288

commit v2 on v1

--- a/solution.py
+++ b/solution.py
@@ -187,26 +187,19 @@
     conv,
     w_sem,
     in_sem,
-    disp_send,
-    disp_recv,
-    xf_send,
+    far_recv,
+    near_recv,
     xf_recv,
-    cf_send,
     cf_recv,
-    r1_send,
+    cw_recv,
     r1_recv,
-    r2_send,
     r2_recv,
-    r3_send,
     r3_recv,
-    r4_send,
     r4_recv,
-    q_send,
     q_recv,
-    ag_send,
     ag_recv,
-    halo_send,
     halo_recv,
+    sent,
 ):
     f32, bf16 = jnp.float32, jnp.bfloat16
     ep = lax.axis_index("ep")
@@ -235,16 +228,15 @@
             src_ref=src, dst_ref=dst, send_sem=send, recv_sem=recv, device_id=to, device_id_type=MESH
         )
 
+    to_send = {
+        name: sent.at[i]
+        for i, name in enumerate(["disp", "core", "pair", "cross", "back", "ag", "q", "halo"])
+    }
+    wing = lax.rem(z, chips // 2)
     core_peer = dev(z, 1 - c, x)
     plane_peer = dev(z, c, 1 - x)
     after = {"ep": lax.rem(ep + 1, n_ep), "tp": x}
     prior = {"ep": lax.rem(ep + n_ep - 1, n_ep), "tp": x}
-    sends = []
-
-    def start(copy):
-        copy.start()
-        sends.append(copy)
-
     barrier = pltpu.get_barrier_semaphore()
     greeted = [core_peer, plane_peer, after, prior] + [dev(peers[k], c, x) for k in range(1, chips)]
     for to in greeted:
@@ -307,37 +299,44 @@
     halo_out[...] = gated.astype(bf16)
 
     pl.semaphore_wait(barrier, len(greeted))
-    halo_copy = remote(halo_out, halo_in, halo_send.at[0], halo_recv.at[0], after)
-    start(halo_copy)
-
-    def dispatch(k, h, s, slot):
-        start(
-            remote(
-                picked.at[k, slot, s],
-                block.at[z, h, s, c],
-                disp_send.at[k, slot, s],
-                disp_recv.at[z, slot, s],
-                dev(peers[k], c, x),
-            )
+    halo_copy = remote(halo_out, halo_in, to_send["halo"], halo_recv.at[0], after)
+    halo_copy.start()
+
+    def far_copy(k, s, at):
+        return remote(
+            picked.at[k, 0, s],
+            block.at[at, x, s, c],
+            to_send["disp"],
+            far_recv.at[lax.rem(at, chips // 2), s],
+            dev(peers[k], c, x),
         )
 
-    def arrived(k, h, s, slot):
-        here = block.at[peers[k], h, s, c]
-        remote(
-            here, here, disp_send.at[k, slot, s], disp_recv.at[peers[k], slot, s], dev(peers[k], c, x)
-        ).wait_recv()
-
-    def to_core(k, h, s):
-        here = block.at[peers[k], h, s, c]
-        start(remote(here, here, cf_send.at[k, h, s], cf_recv.at[k, h, s], core_peer))
-
-    def from_core(k, h, s):
-        here = block.at[peers[k], h, s, 1 - c]
-        remote(here, here, cf_send.at[k, h, s], cf_recv.at[k, h, s], core_peer).wait_recv()
+    def near_dispatch(k, at):
+        return remote(
+            picked.at[k],
+            block.at[at, :, :, c],
+            to_send["disp"],
+            near_recv.at[k - 1],
+            dev(peers[k], c, x),
+        )
+
+    def core_copy(k, h, s, core):
+        here = block.at[peers[k], h, s, core]
+        return remote(here, here, to_send["core"], cf_recv.at[k - split_from, h, s], core_peer)
+
+    def core_copies(k, core):
+        here = block.at[peers[k], :, :, core]
+        return remote(here, here, to_send["core"], cw_recv.at[k], core_peer)
 
     def plane_copy(k, h, s):
         here = block.at[peers[k], h, s, c]
-        return remote(here, here, xf_send.at[k, s], xf_recv.at[k, s], plane_peer)
+        return remote(here, here, to_send["cross"], xf_recv.at[k - split_from, s], plane_peer)
+
+    def from_core(k, h, s):
+        core_copy(k, h, s, 1 - c).wait_recv()
+
+    def slot_of_pair(k, s):
+        return k if k < split_from else split_from + (k - split_from) * subs + s
 
     def pair_copy(k, o, s, n):
         h = x if o else 1 - x
@@ -345,15 +344,19 @@
         return remote(
             part.at[k, 1 - c, h, span],
             pair_in.at[k, h, span],
-            r1_send.at[k, o, s],
-            r1_recv.at[k, o, s],
+            to_send["pair"],
+            r1_recv.at[slot_of_pair(k, s), o],
             core_peer,
         )
 
     def cross_copy(k, s, n):
         span = pl.ds(s * few, n)
         return remote(
-            cross_out.at[k, span], cross_in.at[k, span], r2_send.at[k, s], r2_recv.at[k, s], plane_peer
+            cross_out.at[k, span],
+            cross_in.at[k, span],
+            to_send["cross"],
+            r2_recv.at[k - split_from, s],
+            plane_peer,
         )
 
     def back_copy(k, s, n, at):
@@ -361,8 +364,8 @@
         return remote(
             back_out.at[k, span],
             results.at[at, span],
-            r3_send.at[k, s],
-            r3_recv.at[at, s],
+            to_send["back"],
+            r3_recv.at[lax.rem(at, chips // 2), s],
             dev(peers[k], c, x),
         )
 
@@ -391,7 +394,7 @@
                     for core in range(2):
                         r = (2 * i + core) * few
                         part[k, core, h, cut(s + i), j : j + step] = out[r : r + few]
-            start(pair_copy(k, o, s, n))
+            pair_copy(k, o, s, n).start()
 
     def pair_sum(k, s, n, wait=True):
         if wait:
@@ -399,7 +402,7 @@
         span = slice(s * few, s * few + n)
         total = part[k, c, 1 - x, span].astype(f32) + pair_in[k, 1 - x, span].astype(f32)
         cross_out[k, span] = total.astype(bf16)
-        start(cross_copy(k, s, n))
+        cross_copy(k, s, n).start()
 
     def plane_sum(k, s, n, wait=True):
         if wait:
@@ -412,11 +415,15 @@
             + cross_in[k, span].astype(f32)
         )
         back_out[k, span] = total.astype(bf16)
-        start(back_copy(k, s, n, z))
+        back_copy(k, s, n, z).start()
 
     def near_copy(k, o):
         return remote(
-            near_out.at[k, o], near_res.at[k, o], r4_send.at[k, o], r4_recv.at[k, o], dev(peers[k], c, x)
+            near_out.at[k, o],
+            near_res.at[k, o],
+            to_send["back"],
+            r4_recv.at[k - 1, o],
+            dev(peers[k], c, x),
         )
 
     def near_sum(k, o):
@@ -425,9 +432,9 @@
         total = part[k, c, h].astype(f32) + pair_in[k, h].astype(f32)
         near_out[k, o] = total.astype(bf16)
         if k:
-            start(near_copy(k, o))
-
-    q_copy = remote(q_out, q_in, q_send.at[0], q_recv.at[0], plane_peer)
+            near_copy(k, o).start()
+
+    q_copy = remote(q_out, q_in, to_send["q"], q_recv.at[0], plane_peer)
 
     def close(o):
         total = weighed(0, near_out[0, o])
@@ -438,7 +445,7 @@
             acc[...] = total
         else:
             q_out[...] = total.astype(bf16)
-            start(q_copy)
+            q_copy.start()
 
     def pair_sums(k):
         pair_copy(k, 0, 0, cap).wait_recv()
@@ -453,32 +460,28 @@
     def send_far():
         for s in range(subs):
             for k in far:
-                dispatch(k, x, s, 0)
+                far_copy(k, s, z).start()
 
     def far_in(k, s):
-        arrived(k, x, s, 0)
-        start(plane_copy(k, x, s))
-        to_core(k, x, s)
+        far_copy(k, s, peers[k]).wait_recv()
+        plane_copy(k, x, s).start()
+        core_copy(k, x, s, c).start()
 
     def far_over(k, s):
         plane_copy(k, 1 - x, s).wait_recv()
-        to_core(k, 1 - x, s)
-
-    def far_experts(k, s):
-        for h in range(2):
-            from_core(k, h, s)
-        feed_forward(k, s, few)
+        core_copy(k, 1 - x, s, c).start()
 
     def near_in(k):
-        for h in range(2):
-            for s in range(subs):
-                arrived(k, h, s, h)
-                to_core(k, h, s)
+        near_dispatch(k, peers[k]).wait_recv()
+        core_copies(k, c).start()
 
     def from_cores(k):
-        for h in range(2):
-            for s in range(subs):
-                from_core(k, h, s)
+        if k < split_from:
+            core_copies(k, 1 - c).wait_recv()
+        else:
+            for h in range(2):
+                for s in range(subs):
+                    from_core(k, h, s)
 
     def weighed(k, found):
         return _dot(combs[k, 0], found) + _dot(combs[k, 1], found)
@@ -486,13 +489,19 @@
     rows_per = length // pieces
     tile = 64 if rows_per % 64 == 0 else rows_per
 
-    def gather_copy(p, who):
-        rows_p = conv.at[who, pl.ds(p * rows_per, rows_per)]
-        return remote(rows_p, rows_p, ag_send.at[p], ag_recv.at[p], plane_peer)
+    early = min(pieces, 4)
+    groups = [(p, p + 1) for p in range(1, early)]
+    groups += [(p, min(p + 2, pieces)) for p in range(early, pieces, 2)] + [(0, 1)]
+    gathered = set()
+
+    def gather_copy(g, who):
+        lo, hi = groups[g]
+        rows_g = conv.at[who, pl.ds(lo * rows_per, (hi - lo) * rows_per)]
+        return remote(rows_g, rows_g, to_send["ag"], ag_recv.at[g], plane_peer)
 
     def gather(lo, hi):
-        for p in range(lo, hi):
-            start(gather_copy(p, x))
+        for g in range(lo, hi):
+            gather_copy(g, x).start()
 
     def convolve(lo, hi, send=False):
         def conv_tile(r, carry):
@@ -507,19 +516,20 @@
                     )
                 conv[x, pl.ds(r0, tile), i * LANES : (i + 1) * LANES] = total.astype(bf16)
             if send:
-                gather_copy(r, x).start()
+                rows_r = conv.at[x, pl.ds(r0, tile)]
+                remote(rows_r, rows_r, to_send["ag"], ag_recv.at[r - 1], plane_peer).start()
             return carry
 
         per = rows_per // tile
         send = send and per == 1
         lax.fori_loop(lo * per, hi * per, conv_tile, 0)
-        if send:
-            sends.extend(gather_copy(p, x) for p in range(lo, hi))
         return send
 
     def mix(lo, hi):
-        for p in range(lo, hi):
-            gather_copy(p, 1 - x).wait_recv()
+        for g, (first, last) in enumerate(groups):
+            if g not in gathered and first < hi and last > lo:
+                gather_copy(g, 1 - x).wait_recv()
+                gathered.add(g)
         here = slice(lo * rows_per, hi * rows_per)
         first, second = conv[0, here, :].astype(f32), conv[1, here, :].astype(f32)
         count = 2 * local
@@ -542,16 +552,8 @@
         return acc[...] + weighed(k, results[peers[k]])
 
     def returned(k, n):
-        for s in range(0, cap // few, n // few):
-            zs = peers[k]
-            span = pl.ds(s * few, n)
-            remote(
-                back_out.at[k, span],
-                results.at[zs, span],
-                r3_send.at[k, s],
-                r3_recv.at[zs, s],
-                dev(zs, c, x),
-            ).wait_recv()
+        for s in range(subs):
+            back_copy(k, s, n, peers[k]).wait_recv()
 
     send_far()
     for k in near:
@@ -559,35 +561,23 @@
         for h in range(2):
             for s in range(subs):
                 picked[k, h, s] = rows_k[h][cut(s)]
-                dispatch(k, h, s, h)
+        near_dispatch(k, z).start()
     for h in range(2):
         rows_0 = _dot(pick(0), normed[h]).astype(bf16)
         for s in range(subs):
             block[z, h, s, c] = rows_0[cut(s)]
-    for h in range(2):
-        for s in range(subs):
-            to_core(0, h, s)
+    core_copies(0, c).start()
     kept = slice(0, length - halo)
     for i in range(cols):
         at = slice(i * LANES, (i + 1) * LANES)
         gated = value_ref[kept, at].astype(f32) * jax.nn.sigmoid(gate_ref[kept, at].astype(f32))
         glu[i, halo:length, :] = gated.astype(bf16).astype(f32)
         glu[i, length:, :] = halo_out[:, at].astype(f32)
-    early = min(pieces, 4)
     if not convolve(1, early, True):
-        gather(1, early)
+        gather(0, early - 1)
     convolve(early, pieces)
     mid_far, last_far = far[:-1], far[-1]
     units = [(k, s) for k in mid_far for s in range(subs)]
-    for copy in weights[:3]:
-        copy.wait()
-    from_cores(0)
-    feed_forward(0, 0, cap, lambda: far_in(*units[0]))
-    halo_copy.wait_recv()
-    before = jnp.where(ep > 0, halo_in[...].astype(f32), 0.0)
-    for i in range(cols):
-        glu[i, :halo, :] = before[:, i * LANES : (i + 1) * LANES]
-    convolve(0, 1)
     lane = _iota((tokens, LANES), 1)
     index = _iota((8, tokens), 0)
     rows_named = jnp.where(index == 0, r0t, 0).astype(f32) + jnp.where(index == 1, r1t, 0).astype(f32)
@@ -613,58 +603,84 @@
         combs[k, 1] = (comb - head.astype(f32)).astype(bf16)
 
 
+    halo_copy.wait_recv()
+    before = jnp.where(ep > 0, halo_in[...].astype(f32), 0.0)
+    for i in range(cols):
+        glu[i, :halo, :] = before[:, i * LANES : (i + 1) * LANES]
+    convolve(0, 1)
+    for copy in weights[:3]:
+        copy.wait()
+    from_cores(0)
+    feed_forward(0, 0, cap, lambda: far_in(*units[0]))
     far_over(*units[0])
     for unit in units[1:]:
         far_in(*unit)
-    later = min(pieces, early + 2)
-    gather(early, later)
+    later = min(len(groups), early)
+    gather(early - 1, later)
     for o in range(2):
         near_sum(0, o)
     for h in range(2):
         from_core(units[0][0], h, units[0][1])
-    feed_forward(*units[0], few)
+    feed_forward(*units[0], few, lambda: far_in(last_far, 0))
+
+    def near_ins():
+        for k in near:
+            near_in(k)
+
+    def last_ins():
+        for s in range(1, subs):
+            far_in(last_far, s)
+
+    if len(units) == 1:
+        near_ins()
+        last_ins()
     for i in range(1, len(units)):
         far_over(*units[i])
         pair_sum(*units[i - 1], few)
         for h in range(2):
             from_core(units[i][0], h, units[i][1])
-        feed_forward(*units[i], few, (lambda: far_in(last_far, 0)) if i == 1 else None)
-    if len(units) == 1:
-        far_in(last_far, 0)
-    for k in near:
-        near_in(k)
-    pair_sum(*units[-1], few)
+        only = i == 1
+        feed_forward(*units[i], few, near_ins if only else None, last_ins if only else None)
     far_over(last_far, 0)
-    for s in range(1, subs):
-        far_in(last_far, s)
-    gather(later, pieces)
-    gather(0, 1)
     for k in near:
         from_cores(k)
+
+    def first_back():
+        pair_sum(*units[-1], few)
+        plane_sum(*units[0], few)
+
     for k in near:
-        feed_forward(k, 0, cap, (lambda: plane_sum(*units[0], few)) if k == near[0] else None)
-    for k in near:
-        near_sum(k, 0)
+        feed_forward(k, 0, cap, first_back if k == near[0] else None)
+    gather(later, len(groups))
     for s in range(1, subs):
         far_over(last_far, s)
     for k in near:
-        near_sum(k, 1)
-    for unit in units[1:]:
-        plane_sum(*unit, few)
+        near_sum(k, 0)
     from_cores(last_far)
-    feed_forward(last_far, 0, cap)
+
+    def near_rest():
+        for k in near:
+            near_sum(k, 1)
+
+    def second_back():
+        for unit in units[1:]:
+            plane_sum(*unit, few)
+
+    feed_forward(last_far, 0, cap, near_rest, second_back)
     pair_sums(last_far)
     weights[3].wait()
     group = 2 if pieces % 2 == 0 else 1
-    half = pieces // 2 // group * group
-    for p in range(group, half, group):
+    for p in range(group, pieces, group):
         mix(p, p + group)
-    close(0)
+
+    def close_first():
+        close(0)
+
+    pl.when(swap == 0)(close_first)
     plane_sums(last_far)
+    pl.when(swap == 1)(close_first)
+    mix(0, group)
     close(1)
-    for p in range(max(half, group), pieces, group):
-        mix(p, p + group)
-    mix(0, group)
     for k in far[:-1]:
         returned(k, few)
         acc[...] = combine(k)
@@ -673,8 +689,29 @@
     returned(far[-1], few)
     routed_ref[...] = combine(far[-1]).astype(bf16)
 
-    for copy in sends:
-        copy.wait_send()
+    half = block.at[pl.ds(0, chips // 2)]
+    for name, ref in (
+        ("disp", block.at[0]),
+        ("core", half),
+        ("pair", half),
+        ("cross", block.at[0]),
+        ("back", block.at[0]),
+        ("ag", conv.at[0]),
+        ("q", q_out),
+        ("halo", halo_out),
+    ):
+        remote(ref, ref, to_send[name], halo_recv.at[0], core_peer).wait_send()
+
+
+def store_kernel(mixer_ref, routed_ref, mixer_hbm, routed_hbm, sem):
+    copies = [
+        pltpu.make_async_copy(mixer_ref, mixer_hbm, sem.at[0]),
+        pltpu.make_async_copy(routed_ref, routed_hbm, sem.at[1]),
+    ]
+    for copy in copies:
+        copy.start()
+    for copy in copies:
+        copy.wait()
 
 
 def one_kernel(
@@ -741,28 +778,21 @@
         pltpu.VMEM((2, length, local), bf16),
         dma((4,)),
         dma((8,)),
-        dma((chips, 2, subs)),
-        dma((chips, 2, subs)),
-        dma((chips, subs)),
-        dma((chips, subs)),
-        dma((chips, 2, subs)),
-        dma((chips, 2, subs)),
-        dma((chips, 2, subs)),
-        dma((chips, 2, subs)),
-        dma((chips, subs)),
-        dma((chips, subs)),
-        dma((chips, subs)),
-        dma((chips, subs)),
-        dma((chips // 2, 2)),
-        dma((chips // 2, 2)),
+        dma((chips // 2, subs)),
+        dma((chips // 2 - 1,)),
+        dma((chips // 2, subs)),
+        dma((chips // 2, 2, subs)),
+        dma((chips // 2,)),
+        dma((chips // 2 + (chips // 2 - 1) * subs + 1, 2)),
+        dma((chips // 2, subs)),
+        dma((chips // 2, subs)),
+        dma((chips // 2 - 1, 2)),
         dma((1,)),
+        dma((min(pieces, 4) + (pieces - min(pieces, 4) + 1) // 2,)),
         dma((1,)),
-        dma((pieces,)),
-        dma((pieces,)),
-        dma((1,)),
-        dma((1,)),
+        dma((8,)),
     ]
-    return pl.pallas_call(
+    outs = pl.pallas_call(
         functools.partial(step_kernel, chips, cap, subs, pieces, halo),
         out_shape=(
             jax.ShapeDtypeStruct((length, out_weight.shape[1]), bf16),
@@ -793,11 +823,19 @@
             )
         )
     )
+    return pl.pallas_call(
+        store_kernel,
+        out_shape=tuple(jax.ShapeDtypeStruct(out.shape, out.dtype) for out in outs),
+        in_specs=[vmem] * 2,
+        out_specs=(pl.BlockSpec(memory_space=pl.ANY),) * 2,
+        scratch_shapes=[dma((2,))],
+        compiler_params=pltpu.CompilerParams(vmem_limit_bytes=1024 * 1024),
+    )(*outs)
 
 
 def solution(mesh):
     chips = mesh.shape["ep"] // 2
-    paired = mesh.shape["tp"] == 2 and chips > 1 and chips & (chips - 1) == 0
+    paired = mesh.shape["tp"] == 2 and chips == 4
     placed = (
         P(("grp", "ep"), "tp"),
         P(("grp", "ep"), "tp"),

time: 54.5 us -> 51.6 us (0.947)
  local copies, waits for them, and re-layouts: 1.67 us -> 0 us
  Pallas kernels: 51.4 us -> 50.3 us
    pallas_call x1, Pallas kernels: 51.4 us -> 49.3 us  [one_kernel(): pl.pallas_call(functools.partial(step_kernel, chips, cap, subs, pieces, h...]
    unnamed x2 -> x0, local copies, waits for them, and re-layouts: 1.67 us -> none
    pallas_call x0 -> x1, Pallas kernels: none -> 1.07 us  [one_kernel(): pl.pallas_call(store_kernel, out_shape=tuple((jax.ShapeDtypeStruct(out.sh...]
where the time goes in v2:
time: 51.6 us; the launch traced here: 51.1 us
  Pallas kernels  50.3 us (97%)
  between operations  0.8 us (2%)
    pallas_call x1, Pallas kernels, one_kernel(): pl.pallas_call(functools.partial(step_kernel, chips, cap, subs, pieces, h...  49.3 us
    pallas_call x1, Pallas kernels, one_kernel(): pl.pallas_call(store_kernel, out_shape=tuple((jax.ShapeDtypeStruct(out.sh...  1.07 us

profile of v2, /device:TPU:8, one launch (start us, length us, event | category | flops | bytes accessed | tf_op | source)
XLA Modules:
  0.0 51.1 jit_solution(8931090876775381241)
XLA Ops:
  0.6 49.3 %shard_map.131 = (bf16[512,1024]{1,0:T(8,128)(2,1)S(1)}, bf16[128,1024]{1,0:T(8,128)(2,1)S(1)}) custom-call(bf16[512,512]{1,0:T(8,128)(2,1)} %value_hbm.1, bf16[512,512]{1,0:T(8,128)(2,1)} %gate_hbm.1, f32[31,512]{1,0:T(8,128)} %taps_hbm.1, f32[1,1024]{1,0:T(1,128)} %bitcast.5, bf16[1024,1024]{1,0:T(8,128)(2,1)} %wo_hbm.1, bf16[128,2048]{1,0:T(8,128)(2,1)} %rows_hbm.1, ...), custom_call_target="tpu_custom_call" | custom-call | tf_op jit(solution)/shard_map/pallas_call | solution.py:795
  49.9 1.1 %shard_map.132 = (bf16[512,1024]{1,0:T(8,128)(2,1)}, bf16[128,1024]{1,0:T(8,128)(2,1)}) custom-call(bf16[512,1024]{1,0:T(8,128)(2,1)S(1)} %get-tuple-element.4.mixer_ref, bf16[128,1024]{1,0:T(8,128)(2,1)S(1)} %get-tuple-element.5.routed_ref), custom_call_target="tpu_custom_call" | custom-call | tf_op jit(solution)/shard_map/pallas_call | solution.py:826

commit v3 on v2

--- a/solution.py
+++ b/solution.py
@@ -417,12 +417,15 @@
         back_out[k, span] = total.astype(bf16)
         back_copy(k, s, n, z).start()
 
-    def near_copy(k, o):
+    piece = width // 2
+
+    def near_copy(k, o, j=0):
+        part_cols = pl.ds(0, width) if o else pl.ds(j * piece, piece)
         return remote(
-            near_out.at[k, o],
-            near_res.at[k, o],
+            near_out.at[k, o, :, part_cols],
+            near_res.at[k, o, :, part_cols],
             to_send["back"],
-            r4_recv.at[k - 1, o],
+            r4_recv.at[k - 1, 2 if o else j],
             dev(peers[k], c, x),
         )
 
@@ -432,20 +435,30 @@
         total = part[k, c, h].astype(f32) + pair_in[k, h].astype(f32)
         near_out[k, o] = total.astype(bf16)
         if k:
-            near_copy(k, o).start()
-
-    q_copy = remote(q_out, q_in, to_send["q"], q_recv.at[0], plane_peer)
-
-    def close(o):
-        total = weighed(0, near_out[0, o])
+            for j in range(1 if o else 2):
+                near_copy(k, o, j).start()
+
+    def q_copy(j):
+        part_cols = pl.ds(j * piece, piece)
+        return remote(
+            q_out.at[:, part_cols], q_in.at[:, part_cols], to_send["q"], q_recv.at[j], plane_peer
+        )
+
+    def lend(j):
+        at = slice(j * piece, (j + 1) * piece)
+        total = weighed(0, near_out[0, 0, :, at])
         for k in near:
-            near_copy(k, o).wait_recv()
-            total = total + weighed(k, near_res[k, o])
-        if o:
-            acc[...] = total
-        else:
-            q_out[...] = total.astype(bf16)
-            q_copy.start()
+            near_copy(k, 0, j).wait_recv()
+            total = total + weighed(k, near_res[k, 0, :, at])
+        q_out[:, at] = total.astype(bf16)
+        q_copy(j).start()
+
+    def keep():
+        total = weighed(0, near_out[0, 1])
+        for k in near:
+            near_copy(k, 1).wait_recv()
+            total = total + weighed(k, near_res[k, 1])
+        acc[...] = total
 
     def pair_sums(k):
         pair_copy(k, 0, 0, cap).wait_recv()
@@ -651,40 +664,49 @@
 
     for k in near:
         feed_forward(k, 0, cap, first_back if k == near[0] else None)
-    gather(later, len(groups))
+    gather(later, len(groups) - 1)
     for s in range(1, subs):
         far_over(last_far, s)
-    for k in near:
-        near_sum(k, 0)
-    from_cores(last_far)
-
-    def near_rest():
+
+    def near_sums(o):
         for k in near:
-            near_sum(k, 1)
-
-    def second_back():
-        for unit in units[1:]:
-            plane_sum(*unit, few)
-
-    feed_forward(last_far, 0, cap, near_rest, second_back)
-    pair_sums(last_far)
+            near_sum(k, o)
+
+
+    for s in range(subs):
+        for h in range(2):
+            from_core(last_far, h, s)
+        if s == 0:
+            feed_forward(last_far, s, few, lambda: near_sums(0), lambda: near_sums(1))
+        else:
+            for unit in units[1:] if s == 1 else []:
+                plane_sum(*unit, few)
+            feed_forward(last_far, s, few, lambda: pair_sum(last_far, s - 1, few))
+    pair_sum(last_far, subs - 1, few)
+    gather(len(groups) - 1, len(groups))
     weights[3].wait()
     group = 2 if pieces % 2 == 0 else 1
-    for p in range(group, pieces, group):
+    mix(group, 2 * group)
+    plane_sum(last_far, 0, few)
+    for p in range(2 * group, pieces, group):
         mix(p, p + group)
 
-    def close_first():
-        close(0)
-
-    pl.when(swap == 0)(close_first)
-    plane_sums(last_far)
-    pl.when(swap == 1)(close_first)
+    def lend_all():
+        lend(0)
+        lend(1)
+
+    pl.when(swap == 0)(lend_all)
+    pl.when(swap == 1)(lambda: lend(0))
+    for s in range(1, subs):
+        plane_sum(last_far, s, few)
+    pl.when(swap == 1)(lambda: lend(1))
     mix(0, group)
-    close(1)
+    keep()
     for k in far[:-1]:
         returned(k, few)
         acc[...] = combine(k)
-    q_copy.wait_recv()
+    for j in range(2):
+        q_copy(j).wait_recv()
     acc[...] = acc[...] + q_in[...].astype(f32)
     returned(far[-1], few)
     routed_ref[...] = combine(far[-1]).astype(bf16)
@@ -783,11 +805,11 @@
         dma((chips // 2, subs)),
         dma((chips // 2, 2, subs)),
         dma((chips // 2,)),
-        dma((chips // 2 + (chips // 2 - 1) * subs + 1, 2)),
+        dma((chips // 2 + chips // 2 * subs, 2)),
         dma((chips // 2, subs)),
         dma((chips // 2, subs)),
-        dma((chips // 2 - 1, 2)),
-        dma((1,)),
+        dma((chips // 2 - 1, 3)),
+        dma((2,)),
         dma((min(pieces, 4) + (pieces - min(pieces, 4) + 1) // 2,)),
         dma((1,)),
         dma((8,)),

time: 51.6 us -> 50.7 us (0.983)
    pallas_call x1, Pallas kernels: 49.3 us -> 48.7 us  [one_kernel(): pl.pallas_call(functools.partial(step_kernel, chips, cap, subs, pieces, h...]
where the time goes in v3:
time: 50.7 us; the launch traced here: 50.6 us
  Pallas kernels  49.8 us (98%)
  between operations  0.8 us (2%)
    pallas_call x1, Pallas kernels, one_kernel(): pl.pallas_call(functools.partial(step_kernel, chips, cap, subs, pieces, h...  48.7 us
    pallas_call x1, Pallas kernels, one_kernel(): pl.pallas_call(store_kernel, out_shape=tuple((jax.ShapeDtypeStruct(out.sh...  1.07 us

profile of v3, /device:TPU:8, one launch (start us, length us, event | category | flops | bytes accessed | tf_op | source)
XLA Modules:
  0.0 50.6 jit_solution(8360469977916990543)
XLA Ops:
  0.6 48.7 %shard_map.131 = (bf16[512,1024]{1,0:T(8,128)(2,1)S(1)}, bf16[128,1024]{1,0:T(8,128)(2,1)S(1)}) custom-call(bf16[512,512]{1,0:T(8,128)(2,1)} %value_hbm.1, bf16[512,512]{1,0:T(8,128)(2,1)} %gate_hbm.1, f32[31,512]{1,0:T(8,128)} %taps_hbm.1, f32[1,1024]{1,0:T(1,128)} %bitcast.5, bf16[1024,1024]{1,0:T(8,128)(2,1)} %wo_hbm.1, bf16[128,2048]{1,0:T(8,128)(2,1)} %rows_hbm.1, ...), custom_call_target="tpu_custom_call" | custom-call | tf_op jit(solution)/shard_map/pallas_call | solution.py:817
  49.4 1.1 %shard_map.132 = (bf16[512,1024]{1,0:T(8,128)(2,1)}, bf16[128,1024]{1,0:T(8,128)(2,1)}) custom-call(bf16[512,1024]{1,0:T(8,128)(2,1)S(1)} %get-tuple-element.4.mixer_ref, bf16[128,1024]{1,0:T(8,128)(2,1)S(1)} %get-tuple-element.5.routed_ref), custom_call_target="tpu_custom_call" | custom-call | tf_op jit(solution)/shard_map/pallas_call | solution.py:848

commit v4 on v3

--- a/solution.py
+++ b/solution.py
@@ -243,10 +243,10 @@
         pl.semaphore_signal(barrier, inc=1, device_id=to, device_id_type=MESH)
 
     inputs = [
+        (routes_hbm, routes_t_ref),
         (rows_hbm, rows_ref),
-        (routes_hbm, routes_t_ref),
+        (egain_hbm, egain_ref),
         (rw_hbm, rw_t_ref),
-        (egain_hbm, egain_ref),
         (value_hbm, value_ref),
         (gate_hbm, gate_ref),
         (taps_hbm, taps_ref),
@@ -261,8 +261,7 @@
     ]
     for copy in inputs:
         copy.start()
-    for copy in inputs[:4]:
-        copy.wait()
+    inputs[0].wait()
     erows = -(-chips // 8) * 8
     r0t, r1t = routes_t_ref[0:1, :], routes_t_ref[1:2, :]
     eid = _iota((erows, tokens), 0)
@@ -271,26 +270,28 @@
     place_t = _dot(hits_t.astype(f32).astype(bf16), earlier_t.astype(bf16))
     slot_t = jnp.where(hits_t, place_t, -1.0).astype(jnp.int32)
 
+    slots = _iota((cap, tokens), 0)
+
+    pickers = []
+    for k in range(chips):
+        row = jnp.sum(jnp.where(eid == peers[k], slot_t, 0), axis=0, keepdims=True)
+        pickers.append((slots == row).astype(f32).astype(bf16))
+    for copy in inputs[1:3]:
+        copy.wait()
     rows = rows_ref[...].astype(f32)
     scale = lax.rsqrt(jnp.mean(rows * rows, axis=-1, keepdims=True) + eps)
     both = (rows * scale * egain_ref[...]).astype(bf16)
     normed[0] = both[:, :width]
     normed[1] = both[:, width:]
 
-    slots = _iota((cap, tokens), 0)
-
-    def pick(k):
-        row = jnp.sum(jnp.where(eid == peers[k], slot_t, 0), axis=0, keepdims=True)
-        return (slots == row).astype(f32).astype(bf16)
-
     def cut(s):
         return slice(s * few, (s + 1) * few)
 
     for k in far:
-        rows_k = _dot(pick(k), normed[x]).astype(bf16)
+        rows_k = _dot(pickers[k], normed[x]).astype(bf16)
         for s in range(subs):
             picked[k, 0, s] = rows_k[cut(s)]
-    for copy in inputs[4:]:
+    for copy in inputs[3:]:
         copy.wait()
     for copy in weights:
         copy.start()
@@ -570,13 +571,13 @@
 
     send_far()
     for k in near:
-        rows_k = [_dot(pick(k), normed[h]).astype(bf16) for h in range(2)]
+        rows_k = [_dot(pickers[k], normed[h]).astype(bf16) for h in range(2)]
         for h in range(2):
             for s in range(subs):
                 picked[k, h, s] = rows_k[h][cut(s)]
         near_dispatch(k, z).start()
     for h in range(2):
-        rows_0 = _dot(pick(0), normed[h]).astype(bf16)
+        rows_0 = _dot(pickers[0], normed[h]).astype(bf16)
         for s in range(subs):
             block[z, h, s, c] = rows_0[cut(s)]
     core_copies(0, c).start()
@@ -625,11 +626,11 @@
         copy.wait()
     from_cores(0)
     feed_forward(0, 0, cap, lambda: far_in(*units[0]))
+    later = min(len(groups), early)
+    gather(early - 1, later)
     far_over(*units[0])
     for unit in units[1:]:
         far_in(*unit)
-    later = min(len(groups), early)
-    gather(early - 1, later)
     for o in range(2):
         near_sum(0, o)
     for h in range(2):

time: 50.7 us -> 50.8 us (level)
  no operation moved by 1% of the time
where the time goes in v4:
time: 50.8 us; the launch traced here: 50.7 us
  Pallas kernels  49.9 us (98%)
  between operations  0.8 us (2%)
    pallas_call x1, Pallas kernels, one_kernel(): pl.pallas_call(functools.partial(step_kernel, chips, cap, subs, pieces, h...  48.8 us
    pallas_call x1, Pallas kernels, one_kernel(): pl.pallas_call(store_kernel, out_shape=tuple((jax.ShapeDtypeStruct(out.sh...  1.07 us

profile of v4, /device:TPU:8, one launch (start us, length us, event | category | flops | bytes accessed | tf_op | source)
XLA Modules:
  0.0 50.7 jit_solution(9982196822310737201)
XLA Ops:
  0.6 48.8 %shard_map.131 = (bf16[512,1024]{1,0:T(8,128)(2,1)S(1)}, bf16[128,1024]{1,0:T(8,128)(2,1)S(1)}) custom-call(bf16[512,512]{1,0:T(8,128)(2,1)} %value_hbm.1, bf16[512,512]{1,0:T(8,128)(2,1)} %gate_hbm.1, f32[31,512]{1,0:T(8,128)} %taps_hbm.1, f32[1,1024]{1,0:T(1,128)} %bitcast.5, bf16[1024,1024]{1,0:T(8,128)(2,1)} %wo_hbm.1, bf16[128,2048]{1,0:T(8,128)(2,1)} %rows_hbm.1, ...), custom_call_target="tpu_custom_call" | custom-call | tf_op jit(solution)/shard_map/pallas_call | solution.py:818
  49.4 1.1 %shard_map.132 = (bf16[512,1024]{1,0:T(8,128)(2,1)}, bf16[128,1024]{1,0:T(8,128)(2,1)}) custom-call(bf16[512,1024]{1,0:T(8,128)(2,1)S(1)} %get-tuple-element.4.mixer_ref, bf16[128,1024]{1,0:T(8,128)(2,1)S(1)} %get-tuple-element.5.routed_ref), custom_call_target="tpu_custom_call" | custom-call | tf_op jit(solution)/shard_map/pallas_call | solution.py:849
